TPU v7x, 512 devices: a whole 4x8x8 slice. The times are simulated.
512 devices in a mesh: fs: 64 (over z, y), tp: 8 (over x, core).
Axes of the slice: x: 4, y: 8, z: 8, core: 2. Of those that a mesh axis runs over, the one named last changes fastest.
Arguments:
- inputs: bfloat16 [32768, 2048], P('fs', 'tp'), may hold values from -6 to 6
- value_cotangent: bfloat16 [32768, 2048], P('fs', 'tp'), may hold values from -6 to 6
- first_map: bfloat16 [32768, 2048], P('fs', 'tp'), may hold values from -6 to 6
- second_map: bfloat16 [32768, 2048], P('fs', 'tp'), may hold values from -6 to 6
- lambdas: float32 [16], P('tp'), may hold values from 0.3 to 0.8
- head_gain: float32 [128], replicated, may hold values from 0.1 to 1.9
- output_cotangent: bfloat16 [32768, 2048], P('fs', 'tp'), may hold values from -6 to 6
- value_factor: bfloat16 [2048, 256], replicated, may hold values from -0.125 to 0.125
- output_factor: bfloat16 [2048, 256], replicated, may hold values from -0.125 to 0.125
- value_weight: float32 [2048, 2048], P('fs', 'tp'), may hold values from -0.125 to 0.125
- output_weight: float32 [2048, 2048], P('tp', 'fs'), may hold values from -0.125 to 0.125
- value_moment: float32 [256, 2048], P('fs', 'tp'), may hold values from -6 to 6
- value_second: float32 [256, 2048], P('fs', 'tp'), may hold values from 0.25 to 4
- output_moment: float32 [256, 2048], P('fs', 'tp'), may hold values from -6 to 6
- output_second: float32 [256, 2048], P('fs', 'tp'), may hold values from 0.25 to 4
Outputs:
- value_master: float32 [2048, 2048], P('fs', 'tp')
- output_master: float32 [2048, 2048], P('tp', 'fs')
- value_moment_new: float32 [256, 2048], P('fs', 'tp')
- value_second_new: float32 [256, 2048], P('fs', 'tp')
- output_moment_new: float32 [256, 2048], P('fs', 'tp')
- output_second_new: float32 [256, 2048], P('fs', 'tp')
- value_copy: bfloat16 [2048, 2048], P(None, 'tp')
- output_copy: bfloat16 [2048, 2048], P('tp')
All inputs are finite; a program needn't handle non-finite values.
Results may differ from a plain program's by a relative error of at most 0.0027.
Values may be sent and summed in bfloat16 or wider, within the bound.
No kernel may reach another device: no remote copies, remote signals or barrier semaphores. Data moves between devices by JAX's collectives and lax.ppermute only.
A program may use at most 64 MiB of HBM per device.

v0:
```python
import math
import jax
import jax.numpy as jnp
from jax import lax
from jax.sharding import PartitionSpec as P

F32 = jnp.float32
BF16 = jnp.bfloat16
F16 = jnp.float16
WEIGHT_SCALE = 2.0**18
TOKEN_SCALE = 2.0**4
LOW_SCALE = 2.0 ** (-2)
DIRECTION_SCALE = 2.0**8


def dot(left, right, left_dim, right_dim):
    return lax.dot_general(
        left, right, (((left_dim,), (right_dim,)), ((), ())), preferred_element_type=F32
    )


def two_parts(x):
    high = lax.reduce_precision(x, 8, 7)
    return (high.astype(BF16), (x - high).astype(BF16))


def dot_two(left, right_parts, left_dim, right_dim):
    high, low = right_parts
    return dot(left, high, left_dim, right_dim) + dot(left, low, left_dim, right_dim)


def copy_for_each(x, axis):
    size = lax.axis_size(axis)
    return lax.all_to_all(jnp.broadcast_to(x[None], (size, *x.shape)), axis, 0, 0, tiled=True)


def normed_heads(first_map, second_map, lambdas, head_gain):
    width = head_gain.shape[0]
    heads = []
    for h in range(lambdas.shape[0]):
        cols = slice(h * width, (h + 1) * width)
        difference = first_map[:, cols].astype(F32) - lambdas[h] * second_map[:, cols].astype(F32)
        mean = jnp.mean(difference * difference, axis=-1, keepdims=True)
        heads.append((difference * lax.rsqrt(mean + 1e-06) * head_gain[None, :]).astype(BF16))
    return jnp.concatenate(heads, axis=1)


def local(
    inputs,
    value_cotangent,
    first_map,
    second_map,
    lambdas,
    head_gain,
    output_cotangent,
    value_factor,
    output_factor,
    value_weight,
    output_weight,
    value_moment,
    value_second,
    output_moment,
    output_second,
):
    tok_rows, cols = inputs.shape
    rank = value_factor.shape[1]
    fs_size, tp_size = (lax.axis_size("fs"), lax.axis_size("tp"))
    fs_index, tp_index = (lax.axis_index("fs"), lax.axis_index("tp"))
    width_rows = value_weight.shape[0]
    own_weights = jnp.concatenate([value_weight, output_weight.T], axis=1)
    weights = lax.all_gather((own_weights * WEIGHT_SCALE).astype(F16), "fs", axis=0, tiled=True)
    in_rows = lax.dynamic_slice_in_dim(value_factor, tp_index * cols, cols, 0)
    cot_rows = lax.dynamic_slice_in_dim(output_factor, tp_index * cols, cols, 0)
    projected = jnp.concatenate(
        [dot(inputs, in_rows, 1, 0), dot(output_cotangent, cot_rows, 1, 0)], axis=1
    )
    pieces = (projected * TOKEN_SCALE).astype(F16).reshape(tp_size, -1, 2 * rank)
    pieces = lax.all_to_all(pieces, "tp", 0, 0, tiled=True)
    summed = jnp.sum(pieces.astype(F32), axis=0).astype(F16)
    tokens = copy_for_each(summed, "tp").reshape(tok_rows, 2 * rank).astype(F32)
    heads_out = normed_heads(first_map, second_map, lambdas, head_gain)
    scale = LOW_SCALE / (TOKEN_SCALE * math.sqrt(tok_rows * fs_size))
    token_parts = two_parts(tokens)
    low_value = dot_two(value_cotangent, [p[:, :rank] for p in token_parts], 0, 0)
    low_output = dot_two(heads_out, [p[:, rank:] for p in token_parts], 0, 0)
    partial = jnp.concatenate([low_value.T, low_output.T], axis=1) * scale
    tiles = partial.astype(F16).reshape(fs_size, -1, 2 * cols)
    tiles = lax.all_to_all(tiles, "fs", 0, 0, tiled=True)
    own_rows = jnp.sum(tiles.astype(F32), axis=0) * (1.0 / LOW_SCALE)
    moments = jnp.concatenate([value_moment, output_moment], axis=1)
    seconds = jnp.concatenate([value_second, output_second], axis=1)
    moment_new = 0.8 * moments + 0.2 * own_rows
    second_new = 0.95 * seconds + 0.05 * own_rows * own_rows
    direction = moment_new / (jnp.sqrt(second_new) + 1e-08)
    directions = copy_for_each((direction * DIRECTION_SCALE).astype(F16), "fs")
    parts = two_parts(directions.reshape(rank, 2 * cols).astype(F32))
    value_parts = [p[:, :cols] for p in parts]
    output_parts = [p[:, cols:] for p in parts]
    rate = 0.05 / DIRECTION_SCALE
    value_rows = lax.dynamic_slice_in_dim(value_factor, fs_index * width_rows, width_rows, 0)
    output_rows = lax.dynamic_slice_in_dim(output_factor, fs_index * width_rows, width_rows, 0)
    value_master = value_weight - rate * dot_two(value_rows, value_parts, 1, 0)
    output_master = output_weight - rate * dot_two(output_rows, output_parts, 1, 0).T
    old_value = weights[:, :cols].astype(F32) * (1.0 / WEIGHT_SCALE)
    old_output = weights[:, cols:].T.astype(F32) * (1.0 / WEIGHT_SCALE)
    value_copy = (old_value - rate * dot_two(value_factor, value_parts, 1, 0)).astype(BF16)
    step_output = dot(output_parts[0], output_factor, 0, 1) + dot(
        output_parts[1], output_factor, 0, 1
    )
    output_copy = (old_output - rate * step_output).astype(BF16)
    return (
        value_master,
        output_master,
        moment_new[:, :cols],
        second_new[:, :cols],
        moment_new[:, cols:],
        second_new[:, cols:],
        value_copy,
        output_copy,
    )


def solution(mesh):
    in_specs = (
        P("fs", "tp"),
        P("fs", "tp"),
        P("fs", "tp"),
        P("fs", "tp"),
        P("tp"),
        P(),
        P("fs", "tp"),
        P(),
        P(),
        P("fs", "tp"),
        P("tp", "fs"),
        P("fs", "tp"),
        P("fs", "tp"),
        P("fs", "tp"),
        P("fs", "tp"),
    )
    out_specs = (
        P("fs", "tp"),
        P("tp", "fs"),
        P("fs", "tp"),
        P("fs", "tp"),
        P("fs", "tp"),
        P("fs", "tp"),
        P(None, "tp"),
        P("tp", None),
    )
    return jax.shard_map(local, mesh=mesh, in_specs=in_specs, out_specs=out_specs, check_vma=False)
```

profile of v0, /device:TPU:8, one launch (start us, length us, event | category | flops | bytes accessed | tf_op | source)
XLA Modules:
  0.0 144.4 jit_solution(10989713373295257813)
XLA Ops:
  0.7 1.2 copy-done
  1.9 1.2 convolution_bitcast_fusion.1
  3.3 1.2 convolution_bitcast_fusion
  4.7 0.9 fusion.12
  5.6 4.4 %all-to-all-start = ((f16[8,64,512]{2,1,0:T(8,128)(2,1)}), f16[8,64,512]{2,1,0:T(8,128)(2,1)S(1)}, u32[]{:S(2)}, u32[]{:S(2)}) async-start(f16[8,64,512]{2,1,0:T(8,128)(2,1)} %fusion.12), calls=%async_computation | async-start | bytes 1048576 | tf_op jit(solution)/shard_map/all_to_all | solution.py:78
  10.1 0.6 fusion.55
  10.7 1.5 %multiply_reduce_fusion.1 = (f32[512]{0:T(512)S(1)}, f32[512]{0:T(512)S(1)}) fusion(f32[]{:T(128)} %bitcast.6, bf16[512,256]{1,0:T(8,128)(2,1)S(1)} %copy-done.3, bf16[512,256]{1,0:T(8,128)(2,1)S(1)} %copy-done.4, f32[]{:T(128)} %bitcast.7), kind=kLoop, calls=%fused_computation.42 | loop fusion | flops 785408 | bytes 528392 | tf_op jit(solution)/shard_map/reduce_sum | solution.py:43
  12.2 8.2 %all-to-all-done = f16[8,64,512]{2,1,0:T(8,128)(2,1)S(1)} async-done(((f16[8,64,512]{2,1,0:T(8,128)(2,1)}), f16[8,64,512]{2,1,0:T(8,128)(2,1)S(1)}, u32[]{:S(2)}, u32[]{:S(2)}) %all-to-all-start) | async-done | bytes 524320 | tf_op jit(solution)/shard_map/all_to_all | solution.py:78
  20.5 0.8 broadcast_in_dim.4
  21.3 3.5 %all-to-all-start.1 = ((f16[8,64,512]{2,1,0:T(8,128)(2,1)}), f16[8,64,512]{2,1,0:T(8,128)(2,1)S(1)}, u32[]{:S(2)}, u32[]{:S(2)}) async-start(f16[8,64,512]{2,1,0:T(8,128)(2,1)} %broadcast_in_dim.4), calls=%async_computation.1 | async-start | bytes 1048576 | tf_op jit(solution)/shard_map/all_to_all | solution.py:34
  24.9 1.5 %multiply_convert_fusion.1 = (bf16[512,128]{1,0:T(8,128)(2,1)S(1)}, bf16[512,128]{1,0:T(8,128)(2,1)S(1)}) fusion(f32[128]{0:T(128)S(1)} %copy-done.14, f32[512]{0:T(512)S(1)} %get-tuple-element.52, f32[]{:T(128)} %bitcast.6, bf16[512,256]{1,0:T(8,128)(2,1)S(1)} %copy-done.3, bf16[512,256]{1,0:T(8,128)(2,1)S(1)} %copy-done.4, f32[512]{0:T(512)S(1)} %get-tuple-element.51, ...), kind=kLoop, calls=%fused_computation.41 | loop fusion | flops 917504 | bytes 791048 | tf_op jit(solution)/shard_map/convert_element_type | solution.py:44
  26.4 8.7 %all-to-all-done.1 = f16[8,64,512]{2,1,0:T(8,128)(2,1)S(1)} async-done(((f16[8,64,512]{2,1,0:T(8,128)(2,1)}), f16[8,64,512]{2,1,0:T(8,128)(2,1)S(1)}, u32[]{:S(2)}, u32[]{:S(2)}) %all-to-all-start.1) | async-done | bytes 524320 | tf_op jit(solution)/shard_map/all_to_all | solution.py:34
  35.9 0.3 fusion.19
  36.6 0.9 fusion.14
  37.4 16.6 %all-to-all-start.2 = ((f16[64,4,512]{2,1,0:T(4,128)(2,1)}), f16[64,4,512]{2,1,0:T(4,128)(2,1)S(1)}, u32[]{:S(2)}, u32[]{:S(2)}) async-start(f16[64,4,512]{2,1,0:T(4,128)(2,1)} %fusion.14), calls=%async_computation.2 | async-start | bytes 524288 | tf_op jit(solution)/shard_map/all_to_all | solution.py:88
  54.0 52.9 %all-gather.1 = f16[2048,512]{1,0:T(8,128)(2,1)S(1)} all-gather(f16[32,512]{1,0:T(8,128)(2,1)S(1)} %fusion.35), channel_id=1, replica_groups=mesh['fs'=64,'tp'=8] {'fs'}, dimensions={0}, use_global_device_ids=true | all-gather | bytes 2129920 | tf_op jit(solution)/shard_map/all_gather | solution.py:71
  107.1 0.8 broadcast_in_dim.5
  107.9 10.6 %all-to-all-start.3 = ((f16[64,4,512]{2,1,0:T(4,128)(2,1)}), f16[64,4,512]{2,1,0:T(4,128)(2,1)S(1)}, u32[]{:S(2)}, u32[]{:S(2)}) async-start(f16[64,4,512]{2,1,0:T(4,128)(2,1)} %broadcast_in_dim.5), calls=%async_computation.3 | async-start | bytes 524288 | tf_op jit(solution)/shard_map/all_to_all | solution.py:34
  118.5 1.8 %fusion.52 = (f16[2048,256]{1,0:T(8,128)(2,1)}, f16[2048,256]{1,0:T(8,128)(2,1)}) fusion(f16[2048,512]{1,0:T(8,128)(2,1)S(1)} %all-gather.1), kind=kLoop, calls=%fused_computation.80 | loop fusion | bytes 4194304 | tf_op jit(solution)/shard_map/slice | solution.py:105
  120.3 2.6 %copy.37 = f16[2048,256]{0,1:T(8,128)(2,1)} copy(f16[2048,256]{1,0:T(8,128)(2,1)} %get-tuple-element.37) | data formatting | bytes 2097152
  122.9 1.7 %copy.36 = f16[2048,256]{0,1:T(8,128)(2,1)} copy(f16[2048,256]{1,0:T(8,128)(2,1)S(1)} %copy-done.2) | data formatting | bytes 2097152
  124.6 0.6 fusion.53
  125.2 0.6 fusion.54
  125.8 5.8 %all-to-all-done.3 = f16[64,4,512]{2,1,0:T(4,128)(2,1)S(1)} async-done(((f16[64,4,512]{2,1,0:T(4,128)(2,1)}), f16[64,4,512]{2,1,0:T(4,128)(2,1)S(1)}, u32[]{:S(2)}, u32[]{:S(2)}) %all-to-all-start.3) | async-done | bytes 262176 | tf_op jit(solution)/shard_map/all_to_all | solution.py:34
  132.0 1.7 %fusion.25 = f32[256,2048]{1,0:T(8,128)S(1)} fusion(bf16[2048,256]{1,0:T(8,128)(2,1)} %param.23, bf16[256,512]{1,0:T(8,128)(2,1)S(1)} %get-tuple-element.42), kind=kOutput, calls=%fused_computation.48 | convolution fusion | flops 268435456 | bytes 3276800 | tf_op jit(solution)/shard_map/dot_general | solution.py:17
  133.7 0.5 fusion.31
  134.2 0.9 fusion.27
  135.2 1.6 %fusion.5 = bf16[2048,256]{0,1:T(8,128)(2,1)} fusion(f32[256,2048]{1,0:T(8,128)S(1)} %fusion.31, bf16[2048,256]{1,0:T(8,128)(2,1)S(1)} %copy-done, f16[2048,256]{0,1:T(8,128)(2,1)S(1)} %copy-done.1, bf16[256,512]{1,0:T(8,128)(2,1)S(1)} %get-tuple-element.41), kind=kOutput, calls=%fused_computation.7 | convolution fusion | flops 271581184 | bytes 5373952 | tf_op jit(solution)/shard_map/dot_general | solution.py:17
  136.8 2.3 %copy.35 = bf16[2048,256]{1,0:T(8,128)(2,1)} copy(bf16[2048,256]{0,1:T(8,128)(2,1)} %fusion.5) | data formatting | bytes 2097152
  139.1 1.5 %fusion.8 = f32[256,32]{0,1:T(8,128)} fusion(f32[256,32]{0,1:T(8,128)S(1)} %copy-done.7, f32[256,32]{0,1:T(8,128)S(1)} %fusion.27, bf16[256,512]{1,0:T(8,128)(2,1)S(1)} %get-tuple-element.41, bf16[2048,256]{1,0:T(8,128)(2,1)} %param.23, s32[]{:T(128)S(6)} %select_n.8), kind=kOutput, calls=%fused_computation.17 | convolution fusion | flops 4218880 | bytes 245764 | tf_op jit(solution)/shard_map/dot_general | solution.py:17
  140.6 0.8 fusion.10
  141.3 3.1 %fusion.6 = bf16[256,2048]{1,0:T(8,128)(2,1)} fusion(f32[256,2048]{1,0:T(8,128)S(1)} %fusion.25, bf16[2048,256]{1,0:T(8,128)(2,1)} %param.23, f16[2048,256]{0,1:T(8,128)(2,1)} %copy.37, bf16[256,512]{1,0:T(8,128)(2,1)S(1)} %get-tuple-element.41), kind=kOutput, calls=%fused_computation.8 | convolution fusion | flops 271581184 | bytes 5373952 | tf_op jit(solution)/shard_map/dot_general | solution.py:17
  (48 shorter events, 2.4 us)
Async XLA Ops:
  0.6 1.2 copy-start
  0.6 2.6 %copy-start.6 = (bf16[512,256]{1,0:T(8,128)(2,1)S(1)}, bf16[512,256]{1,0:T(8,128)(2,1)}, u32[]{:S(2)}) copy-start(bf16[512,256]{1,0:T(8,128)(2,1)} %param.21) | copy-start | bytes 786436
  3.3 6.8 %copy-start.13 = (f32[2]{0:T(128)S(1)}, f32[2]{0:T(128)}, u32[]{:S(2)}) copy-start(f32[2]{0:T(128)} %param.19) | copy-start | bytes 28
  3.3 7.4 %copy-start.7 = (f32[256,32]{0,1:T(8,128)S(1)}, f32[256,32]{0,1:T(8,128)}, u32[]{:S(2)}) copy-start(f32[256,32]{0,1:T(8,128)} %param.25) | copy-start | bytes 98308
  3.3 7.3 %copy-start.8 = (f32[32,256]{1,0:T(8,128)S(1)}, f32[32,256]{1,0:T(8,128)}, u32[]{:S(2)}) copy-start(f32[32,256]{1,0:T(8,128)} %param.24) | copy-start | bytes 98308
  4.5 6.2 %copy-start.3 = (bf16[512,256]{1,0:T(8,128)(2,1)S(1)}, bf16[512,256]{1,0:T(8,128)(2,1)}, u32[]{:S(2)}) copy-start(bf16[512,256]{1,0:T(8,128)(2,1)} %param.18) | copy-start | bytes 786436
  4.5 6.2 %copy-start.4 = (bf16[512,256]{1,0:T(8,128)(2,1)S(1)}, bf16[512,256]{1,0:T(8,128)(2,1)}, u32[]{:S(2)}) copy-start(bf16[512,256]{1,0:T(8,128)(2,1)} %param.17) | copy-start | bytes 786436
  5.6 19.2 %copy-start.14 = (f32[128]{0:T(128)S(1)}, f32[128]{0:T(128)}, u32[]{:S(2)}) copy-start(f32[128]{0:T(128)} %param.20) | copy-start | bytes 1540
  5.6 14.7 %all-to-all-start = ((f16[8,64,512]{2,1,0:T(8,128)(2,1)}), f16[8,64,512]{2,1,0:T(8,128)(2,1)S(1)}, u32[]{:S(2)}, u32[]{:S(2)}) async-start(f16[8,64,512]{2,1,0:T(8,128)(2,1)} %fusion.12), calls=%async_computation | async-start | bytes 1048576 | tf_op jit(solution)/shard_map/all_to_all | solution.py:78
  21.3 13.7 %all-to-all-start.1 = ((f16[8,64,512]{2,1,0:T(8,128)(2,1)}), f16[8,64,512]{2,1,0:T(8,128)(2,1)S(1)}, u32[]{:S(2)}, u32[]{:S(2)}) async-start(f16[8,64,512]{2,1,0:T(8,128)(2,1)} %broadcast_in_dim.4), calls=%async_computation.1 | async-start | bytes 1048576 | tf_op jit(solution)/shard_map/all_to_all | solution.py:34
  26.4 9.5 %copy-start.5 = (bf16[512,256]{1,0:T(8,128)(2,1)S(1)}, bf16[512,256]{1,0:T(8,128)(2,1)}, u32[]{:S(2)}) copy-start(bf16[512,256]{1,0:T(8,128)(2,1)} %param.16) | copy-start | bytes 786436
  36.4 70.6 %copy-start.9 = (f32[4,256]{1,0:T(4,128)S(1)}, f32[4,256]{1,0:T(4,128)}, u32[]{:S(2)}) copy-start(f32[4,256]{1,0:T(4,128)} %param.29) | copy-start | bytes 12292
  36.5 70.6 %copy-start.10 = (f32[4,256]{1,0:T(4,128)S(1)}, f32[4,256]{1,0:T(4,128)}, u32[]{:S(2)}) copy-start(f32[4,256]{1,0:T(4,128)} %param.27) | copy-start | bytes 12292
  36.5 70.6 %copy-start.11 = (f32[4,256]{1,0:T(4,128)S(1)}, f32[4,256]{1,0:T(4,128)}, u32[]{:S(2)}) copy-start(f32[4,256]{1,0:T(4,128)} %param.28) | copy-start | bytes 12292
  36.5 70.6 %copy-start.12 = (f32[4,256]{1,0:T(4,128)S(1)}, f32[4,256]{1,0:T(4,128)}, u32[]{:S(2)}) copy-start(f32[4,256]{1,0:T(4,128)} %param.26) | copy-start | bytes 12292
  37.4 69.5 %all-to-all-start.2 = ((f16[64,4,512]{2,1,0:T(4,128)(2,1)}), f16[64,4,512]{2,1,0:T(4,128)(2,1)S(1)}, u32[]{:S(2)}, u32[]{:S(2)}) async-start(f16[64,4,512]{2,1,0:T(4,128)(2,1)} %fusion.14), calls=%async_computation.2 | async-start | bytes 524288 | tf_op jit(solution)/shard_map/all_to_all | solution.py:88
  107.9 23.7 %all-to-all-start.3 = ((f16[64,4,512]{2,1,0:T(4,128)(2,1)}), f16[64,4,512]{2,1,0:T(4,128)(2,1)S(1)}, u32[]{:S(2)}, u32[]{:S(2)}) async-start(f16[64,4,512]{2,1,0:T(4,128)(2,1)} %broadcast_in_dim.5), calls=%async_computation.3 | async-start | bytes 524288 | tf_op jit(solution)/shard_map/all_to_all | solution.py:34
  120.3 2.6 %copy-start.2 = (f16[2048,256]{1,0:T(8,128)(2,1)S(1)}, f16[2048,256]{1,0:T(8,128)(2,1)}, u32[]{:S(2)}) copy-start(f16[2048,256]{1,0:T(8,128)(2,1)} %get-tuple-element.38) | copy-start | bytes 3145732
  133.7 1.5 %copy-start.1 = (f16[2048,256]{0,1:T(8,128)(2,1)S(1)}, f16[2048,256]{0,1:T(8,128)(2,1)}, u32[]{:S(2)}) copy-start(f16[2048,256]{0,1:T(8,128)(2,1)} %copy.36) | copy-start | bytes 3145732
where the time goes:
time: 145 us; the launch traced here: 144 us
  blocking collectives  52.9 us (36%)
  starting transfers between devices  35.1 us (24%)
  waiting for transfers between devices  22.7 us (16%)
  local copies, waits for them, and re-layouts  13.7 us (9%)
  matrix products  13.7 us (9%)
  other arithmetic  5.39 us (4%)
    all_gather x1, blocking collectives, local(): lax.all_gather((own_weights * WEIGHT_SCALE).astype(F16), 'fs', axis=0, ti...  52.9 us
    all_to_all x1, starting transfers between devices, local(): tiles = lax.all_to_all(tiles, 'fs', 0, 0, tiled=True)  16.6 us
    all_to_all x2, waiting for transfers between devices, copy_for_each(): lax.all_to_all(jnp.broadcast_to(x[None], (size, *x.shape)), axis, 0, 0, t...  14.5 us
    all_to_all x2, starting transfers between devices, copy_for_each(): lax.all_to_all(jnp.broadcast_to(x[None], (size, *x.shape)), axis, 0, 0, t...  14.1 us
    dot_general x14, matrix products, dot(): lax.dot_general(left, right, (((left_dim,), (right_dim,)), ((), ())), pre...  13.7 us
    all_to_all x1, waiting for transfers between devices, local(): pieces = lax.all_to_all(pieces, 'tp', 0, 0, tiled=True)  8.17 us
    unnamed x33, local copies, waits for them, and re-layouts  7.84 us
    all_to_all x1, starting transfers between devices, local(): pieces = lax.all_to_all(pieces, 'tp', 0, 0, tiled=True)  4.43 us
  transfers between devices with their start and end apart: 4, of which 3 were waited for; matrix products, arithmetic and copies ran while one was open for 8% of the time, Pallas kernels for 0%

commit v1 on v0

--- a/solution.py
+++ b/solution.py
@@ -1,8 +1,10 @@
+import functools
 import math
 import jax
 import jax.numpy as jnp
 from jax import lax
 from jax.sharding import PartitionSpec as P
+from jax.lax import all_to_all, psum
 
 F32 = jnp.float32
 BF16 = jnp.bfloat16
@@ -11,6 +13,17 @@
 TOKEN_SCALE = 2.0**4
 LOW_SCALE = 2.0 ** (-2)
 DIRECTION_SCALE = 2.0**8
+
+
+def load_the_panels(message, lane_axis):
+    copies = []
+    for _ in range(psum(1, lane_axis)):
+        copies.append(message)
+    wide_out = jnp.concatenate(copies, axis=0)
+    return all_to_all(wide_out, lane_axis, 0, 0, tiled=True)
+
+
+recast_the_record = functools.partial(load_the_panels, lane_axis="fs")
 
 
 def dot(left, right, left_dim, right_dim):
@@ -68,7 +81,7 @@
     fs_index, tp_index = (lax.axis_index("fs"), lax.axis_index("tp"))
     width_rows = value_weight.shape[0]
     own_weights = jnp.concatenate([value_weight, output_weight.T], axis=1)
-    weights = lax.all_gather((own_weights * WEIGHT_SCALE).astype(F16), "fs", axis=0, tiled=True)
+    weights = recast_the_record((own_weights * WEIGHT_SCALE).astype(F16))
     in_rows = lax.dynamic_slice_in_dim(value_factor, tp_index * cols, cols, 0)
     cot_rows = lax.dynamic_slice_in_dim(output_factor, tp_index * cols, cols, 0)
     projected = jnp.concatenate(

time: 145 us -> 170 us (1.17)
  waiting for transfers between devices: 22.7 us -> 78.6 us
  blocking collectives: 52.9 us -> 0 us
  matrix products: 13.7 us -> 20.7 us
  local copies, waits for them, and re-layouts: 13.7 us -> 20.7 us
  other arithmetic: 5.39 us -> 12 us
    all_gather x1 -> x0, blocking collectives: 52.9 us -> none  [local(): lax.all_gather((own_weights * WEIGHT_SCALE).astype(F16), 'fs', axis=0, ti...]
    all_to_all x0 -> x1, waiting for transfers between devices: none -> 37.1 us  [load_the_panels(): return all_to_all(wide_out, lane_axis, 0, 0, tiled=True)]
    all_to_all x1, waiting for transfers between devices: 0.01 us -> 13.9 us  [local(): tiles = lax.all_to_all(tiles, 'fs', 0, 0, tiled=True)]
    dot_general x14, matrix products: 13.7 us -> 20.7 us  [dot(): lax.dot_general(left, right, (((left_dim,), (right_dim,)), ((), ())), pre...]
    all_to_all x2, waiting for transfers between devices: 14.5 us -> 20.3 us  [copy_for_each(): lax.all_to_all(jnp.broadcast_to(x[None], (size, *x.shape)), axis, 0, 0, t...]
    all_to_all x0 -> x1, starting transfers between devices: none -> 5.34 us  [load_the_panels(): return all_to_all(wide_out, lane_axis, 0, 0, tiled=True)]
    all_to_all x2, starting transfers between devices: 14.1 us -> 9.27 us  [copy_for_each(): lax.all_to_all(jnp.broadcast_to(x[None], (size, *x.shape)), axis, 0, 0, t...]
    concatenate x2, local copies, waits for them, and re-layouts: 0.15 us -> 2.75 us  [local(): partial = jnp.concatenate([low_value.T, low_output.T], axis=1) * scale]
  transfers between devices with their start and end apart: 4 -> 5, of which waited for: 3 -> 5; matrix products, arithmetic and copies ran while one was open for 8% -> 11% of each run, Pallas kernels for 0% -> 0%
where the time goes in v1:
time: 170 us; the launch traced here: 169 us
  waiting for transfers between devices  78.6 us (46%)
  starting transfers between devices  35.6 us (21%)
  local copies, waits for them, and re-layouts  20.7 us (12%)
  matrix products  20.7 us (12%)
  other arithmetic  12 us (7%)
    all_to_all x1, waiting for transfers between devices, load_the_panels(): return all_to_all(wide_out, lane_axis, 0, 0, tiled=True)  37.1 us
    dot_general x14, matrix products, dot(): lax.dot_general(left, right, (((left_dim,), (right_dim,)), ((), ())), pre...  20.7 us
    all_to_all x2, waiting for transfers between devices, copy_for_each(): lax.all_to_all(jnp.broadcast_to(x[None], (size, *x.shape)), axis, 0, 0, t...  20.3 us
    all_to_all x1, starting transfers between devices, local(): tiles = lax.all_to_all(tiles, 'fs', 0, 0, tiled=True)  16.6 us
    all_to_all x1, waiting for transfers between devices, local(): tiles = lax.all_to_all(tiles, 'fs', 0, 0, tiled=True)  13.9 us
    unnamed x105, local copies, waits for them, and re-layouts  10.3 us
    all_to_all x2, starting transfers between devices, copy_for_each(): lax.all_to_all(jnp.broadcast_to(x[None], (size, *x.shape)), axis, 0, 0, t...  9.27 us
    all_to_all x1, waiting for transfers between devices, local(): pieces = lax.all_to_all(pieces, 'tp', 0, 0, tiled=True)  7.26 us
  transfers between devices with their start and end apart: 5, of which 5 were waited for; matrix products, arithmetic and copies ran while one was open for 11% of the time, Pallas kernels for 0%

profile of v1, /device:TPU:8, one launch (start us, length us, event | category | flops | bytes accessed | tf_op | source)
XLA Modules:
  0.0 169.1 jit_solution(17143054463755780011)
XLA Ops:
  0.7 1.2 copy-done
  1.9 1.2 convolution_bitcast_fusion.1
  3.3 1.2 convolution_bitcast_fusion
  5.6 4.4 %all-to-all-start = ((f16[8,64,512]{2,1,0:T(8,128)(2,1)}), f16[8,64,512]{2,1,0:T(8,128)(2,1)}, u32[]{:S(2)}, u32[]{:S(2)}) async-start(f16[8,64,512]{2,1,0:T(8,128)(2,1)} %fusion.12), calls=%async_computation | async-start | bytes 1048576 | tf_op jit(solution)/shard_map/all_to_all | solution.py:91
  11.7 1.5 multiply_reduce_fusion.1
  13.2 7.3 %all-to-all-done = f16[8,64,512]{2,1,0:T(8,128)(2,1)} async-done(((f16[8,64,512]{2,1,0:T(8,128)(2,1)}), f16[8,64,512]{2,1,0:T(8,128)(2,1)}, u32[]{:S(2)}, u32[]{:S(2)}) %all-to-all-start) | async-done | bytes 524320 | tf_op jit(solution)/shard_map/all_to_all | solution.py:91
  22.5 4.1 %all-to-all-start.1 = ((f16[8,64,512]{2,1,0:T(8,128)(2,1)}), f16[8,64,512]{2,1,0:T(8,128)(2,1)}, u32[]{:S(2)}, u32[]{:S(2)}) async-start(f16[8,64,512]{2,1,0:T(8,128)(2,1)} %broadcast_in_dim.4), calls=%async_computation.1 | async-start | bytes 1048576 | tf_op jit(solution)/shard_map/all_to_all | solution.py:47
  26.6 3.2 %multiply_convert_fusion.1 = (bf16[512,128]{1,0:T(8,128)(2,1)}, bf16[512,128]{1,0:T(8,128)(2,1)}) fusion(f32[128]{0:T(128)S(1)} %copy-done.19, f32[512]{0:T(512)S(1)} %get-tuple-element.46, f32[]{:T(128)} %bitcast.6, bf16[512,256]{1,0:T(8,128)(2,1)S(1)} %copy-done.7, bf16[512,256]{1,0:T(8,128)(2,1)} %param.17, f32[512]{0:T(512)S(1)} %get-tuple-element.45, ...), kind=kLoop, calls=%fused_computation.41 | loop fusion | flops 917504 | bytes 791048 | tf_op jit(solution)/shard_map/convert_element_type | solution.py:57
  29.8 7.1 %all-to-all-done.1 = f16[8,64,512]{2,1,0:T(8,128)(2,1)} async-done(((f16[8,64,512]{2,1,0:T(8,128)(2,1)}), f16[8,64,512]{2,1,0:T(8,128)(2,1)}, u32[]{:S(2)}, u32[]{:S(2)}) %all-to-all-start.1) | async-done | bytes 524320 | tf_op jit(solution)/shard_map/all_to_all | solution.py:47
  36.9 1.2 fusion.11
  38.9 1.2 fusion.16
  42.2 1.3 fusion.19
  43.5 2.0 %convolution_add_fusion.3 = f32[256,256]{1,0:T(8,128)} fusion(f32[256,256]{1,0:T(8,128)S(1)} %fusion.19, bf16[512,256]{1,0:T(8,128)(2,1)} %param.16, bf16[512,512]{1,0:T(8,128)(2,1)} %copy-done.6), kind=kOutput, calls=%fused_computation.14 | convolution fusion | flops 67174400 | bytes 1048576 | tf_op jit(solution)/shard_map/dot_general | solution.py:30
  45.5 1.7 %concatenate.43 = f32[64,4,256]{2,1,0:T(4,128)} reshape(f32[256,256]{1,0:T(8,128)} %convolution_add_fusion.3) | data formatting | bytes 524288 | tf_op jit(solution)/shard_map/concatenate | solution.py:99
  47.3 1.8 %fusion.14 = f16[64,4,512]{2,1,0:T(4,128)(2,1)} fusion(f32[64,4,256]{2,1,0:T(4,128)S(1)} %concatenate.45, f32[64,4,256]{2,1,0:T(4,128)} %concatenate.43), kind=kLoop, calls=%fused_computation.29 | loop fusion | flops 393216 | bytes 786432 | tf_op jit(solution)/shard_map/convert_element_type | solution.py:100
  49.1 16.6 %all-to-all-start.2 = ((f16[64,4,512]{2,1,0:T(4,128)(2,1)}), f16[64,4,512]{2,1,0:T(4,128)(2,1)S(1)}, u32[]{:S(2)}, u32[]{:S(2)}) async-start(f16[64,4,512]{2,1,0:T(4,128)(2,1)} %fusion.14), calls=%async_computation.2 | async-start | bytes 524288 | tf_op jit(solution)/shard_map/all_to_all | solution.py:101
  65.8 13.9 %all-to-all-done.2 = f16[64,4,512]{2,1,0:T(4,128)(2,1)S(1)} async-done(((f16[64,4,512]{2,1,0:T(4,128)(2,1)}), f16[64,4,512]{2,1,0:T(4,128)(2,1)S(1)}, u32[]{:S(2)}, u32[]{:S(2)}) %all-to-all-start.2) | async-done | bytes 262176 | tf_op jit(solution)/shard_map/all_to_all | solution.py:101
  80.7 5.1 %all-to-all-start.3 = ((f16[64,4,512]{2,1,0:T(4,128)(2,1)}), f16[64,4,512]{2,1,0:T(4,128)(2,1)S(1)}, u32[]{:S(2)}, u32[]{:S(2)}) async-start(f16[64,4,512]{2,1,0:T(4,128)(2,1)} %broadcast_in_dim.5), calls=%async_computation.3 | async-start | bytes 524288 | tf_op jit(solution)/shard_map/all_to_all | solution.py:47
  85.9 13.2 %all-to-all-done.3 = f16[64,4,512]{2,1,0:T(4,128)(2,1)S(1)} async-done(((f16[64,4,512]{2,1,0:T(4,128)(2,1)}), f16[64,4,512]{2,1,0:T(4,128)(2,1)S(1)}, u32[]{:S(2)}, u32[]{:S(2)}) %all-to-all-start.3) | async-done | bytes 262176 | tf_op jit(solution)/shard_map/all_to_all | solution.py:47
  99.1 5.3 %all-to-all-start.4 = ((f16[64,32,512]{2,1,0:T(8,128)(2,1)}), f16[64,32,512]{2,1,0:T(8,128)(2,1)S(1)}, u32[]{:S(2)}, u32[]{:S(2)}) async-start(f16[64,32,512]{2,1,0:T(8,128)(2,1)} %bitcast.32), calls=%async_computation.4 | async-start | bytes 4194304 | tf_op jit(solution)/shard_map/all_to_all | solution.py:23
  106.5 2.0 %reshape.94 = f32[256,512]{1,0:T(8,128)} reshape(f32[64,4,512]{2,1,0:T(4,128)} %convert_element_type.112) | data formatting | bytes 1048576 | tf_op jit(solution)/shard_map/convert_element_type | solution.py:109
  108.5 1.2 fusion.13
  110.7 1.5 fusion.8
  113.0 1.8 %fusion.25 = f32[256,2048]{1,0:T(8,128)} fusion(bf16[2048,256]{1,0:T(8,128)(2,1)S(1)} %copy-done.3, bf16[256,512]{1,0:T(8,128)(2,1)S(1)} %get-tuple-element.36), kind=kOutput, calls=%fused_computation.112 | convolution fusion | flops 268435456 | bytes 3276800 | tf_op jit(solution)/shard_map/dot_general | solution.py:30
  114.8 1.8 %fusion.31 = f32[256,2048]{1,0:T(8,128)} fusion(bf16[2048,256]{1,0:T(8,128)(2,1)S(1)} %copy-done, bf16[256,512]{1,0:T(8,128)(2,1)S(1)} %get-tuple-element.36), kind=kOutput, calls=%fused_computation.118 | convolution fusion | flops 268435456 | bytes 3276800 | tf_op jit(solution)/shard_map/dot_general | solution.py:30
  116.6 37.1 %all-to-all-done.4 = f16[64,32,512]{2,1,0:T(8,128)(2,1)S(1)} async-done(((f16[64,32,512]{2,1,0:T(8,128)(2,1)}), f16[64,32,512]{2,1,0:T(8,128)(2,1)S(1)}, u32[]{:S(2)}, u32[]{:S(2)}) %all-to-all-start.4) | async-done | bytes 2097184 | tf_op jit(solution)/shard_map/all_to_all | solution.py:23
  153.8 1.8 %fusion.53 = (f16[2048,256]{1,0:T(8,128)(2,1)}, f16[2048,256]{1,0:T(8,128)(2,1)}) fusion(f16[2048,512]{1,0:T(8,128)(2,1)S(1)} %bitcast.31), kind=kLoop, calls=%fused_computation.144 | loop fusion | bytes 4194304 | tf_op jit(solution)/shard_map/slice | solution.py:118
  155.5 2.7 %copy.31 = f16[2048,256]{0,1:T(8,128)(2,1)} copy(f16[2048,256]{1,0:T(8,128)(2,1)} %get-tuple-element.31) | data formatting | bytes 2097152
  158.2 2.5 %copy.30 = f16[2048,256]{0,1:T(8,128)(2,1)} copy(f16[2048,256]{1,0:T(8,128)(2,1)} %get-tuple-element.32) | data formatting | bytes 2097152
  160.7 2.8 %fusion.5 = bf16[2048,256]{0,1:T(8,128)(2,1)} fusion(f32[256,2048]{1,0:T(8,128)S(1)} %copy-done.2, bf16[2048,256]{1,0:T(8,128)(2,1)S(1)} %copy-done, f16[2048,256]{0,1:T(8,128)(2,1)} %copy.30, bf16[256,512]{1,0:T(8,128)(2,1)S(1)} %get-tuple-element.35), kind=kOutput, calls=%fused_computation.7 | convolution fusion | flops 271581184 | bytes 5373952 | tf_op jit(solution)/shard_map/dot_general | solution.py:30
  163.5 2.4 %copy.29 = bf16[2048,256]{1,0:T(8,128)(2,1)} copy(bf16[2048,256]{0,1:T(8,128)(2,1)} %fusion.5) | data formatting | bytes 2097152
  165.9 3.1 %fusion.6 = bf16[256,2048]{1,0:T(8,128)(2,1)} fusion(f32[256,2048]{1,0:T(8,128)S(1)} %copy-done.1, bf16[2048,256]{1,0:T(8,128)(2,1)} %param.23, f16[2048,256]{0,1:T(8,128)(2,1)} %copy.31, bf16[256,512]{1,0:T(8,128)(2,1)S(1)} %get-tuple-element.35), kind=kOutput, calls=%fused_computation.8 | convolution fusion | flops 271581184 | bytes 5373952 | tf_op jit(solution)/shard_map/dot_general | solution.py:30
  (122 shorter events, 12.2 us)
Async XLA Ops:
  0.6 1.2 copy-start
  0.6 2.6 %copy-start.9 = (bf16[512,256]{1,0:T(8,128)(2,1)S(1)}, bf16[512,256]{1,0:T(8,128)(2,1)}, u32[]{:S(2)}) copy-start(bf16[512,256]{1,0:T(8,128)(2,1)} %param.21) | copy-start | bytes 786436
  3.3 6.7 %copy-start.10 = (f32[256,32]{0,1:T(8,128)S(1)}, f32[256,32]{0,1:T(8,128)}, u32[]{:S(2)}) copy-start(f32[256,32]{0,1:T(8,128)} %param.25) | copy-start | bytes 98308
  3.3 6.7 %copy-start.11 = (f32[32,256]{1,0:T(8,128)S(1)}, f32[32,256]{1,0:T(8,128)}, u32[]{:S(2)}) copy-start(f32[32,256]{1,0:T(8,128)} %param.24) | copy-start | bytes 98308
  5.6 5.4 %copy-start.18 = (f32[2]{0:T(128)S(1)}, f32[2]{0:T(128)}, u32[]{:S(2)}) copy-start(f32[2]{0:T(128)} %param.19) | copy-start | bytes 28
  5.6 6.1 %copy-start.7 = (bf16[512,256]{1,0:T(8,128)(2,1)S(1)}, bf16[512,256]{1,0:T(8,128)(2,1)}, u32[]{:S(2)}) copy-start(bf16[512,256]{1,0:T(8,128)(2,1)} %param.18) | copy-start | bytes 786436
  5.6 14.9 %all-to-all-start = ((f16[8,64,512]{2,1,0:T(8,128)(2,1)}), f16[8,64,512]{2,1,0:T(8,128)(2,1)}, u32[]{:S(2)}, u32[]{:S(2)}) async-start(f16[8,64,512]{2,1,0:T(8,128)(2,1)} %fusion.12), calls=%async_computation | async-start | bytes 1048576 | tf_op jit(solution)/shard_map/all_to_all | solution.py:91
  10.0 1.6 copy-start.8
  10.7 15.9 %copy-start.19 = (f32[128]{0:T(128)S(1)}, f32[128]{0:T(128)}, u32[]{:S(2)}) copy-start(f32[128]{0:T(128)} %param.20) | copy-start | bytes 1540
  22.5 14.5 %all-to-all-start.1 = ((f16[8,64,512]{2,1,0:T(8,128)(2,1)}), f16[8,64,512]{2,1,0:T(8,128)(2,1)}, u32[]{:S(2)}, u32[]{:S(2)}) async-start(f16[8,64,512]{2,1,0:T(8,128)(2,1)} %broadcast_in_dim.4), calls=%async_computation.1 | async-start | bytes 1048576 | tf_op jit(solution)/shard_map/all_to_all | solution.py:47
  29.8 10.4 %copy-start.12 = (bf16[512,128]{1,0:T(8,128)(2,1)S(1)}, bf16[512,128]{1,0:T(8,128)(2,1)}, u32[]{:S(2)}) copy-start(bf16[512,128]{1,0:T(8,128)(2,1)} %get-tuple-element.33) | copy-start | bytes 393220
  29.8 10.4 %copy-start.13 = (bf16[512,128]{1,0:T(8,128)(2,1)S(1)}, bf16[512,128]{1,0:T(8,128)(2,1)}, u32[]{:S(2)}) copy-start(bf16[512,128]{1,0:T(8,128)(2,1)} %get-tuple-element.34) | copy-start | bytes 393220
  38.1 0.8 copy-start.5
  38.1 2.0 %copy-start.6 = (bf16[512,512]{1,0:T(8,128)(2,1)}, bf16[512,512]{1,0:T(8,128)(2,1)S(1)}, u32[]{:S(2)}) copy-start(bf16[512,512]{1,0:T(8,128)(2,1)S(1)} %get-tuple-element.37) | copy-start | bytes 1572868
  42.2 37.7 %copy-start.14 = (f32[4,256]{1,0:T(4,128)S(1)}, f32[4,256]{1,0:T(4,128)}, u32[]{:S(2)}) copy-start(f32[4,256]{1,0:T(4,128)} %param.29) | copy-start | bytes 12292
  42.2 37.6 %copy-start.15 = (f32[4,256]{1,0:T(4,128)S(1)}, f32[4,256]{1,0:T(4,128)}, u32[]{:S(2)}) copy-start(f32[4,256]{1,0:T(4,128)} %param.27) | copy-start | bytes 12292
  42.2 37.6 %copy-start.16 = (f32[4,256]{1,0:T(4,128)S(1)}, f32[4,256]{1,0:T(4,128)}, u32[]{:S(2)}) copy-start(f32[4,256]{1,0:T(4,128)} %param.28) | copy-start | bytes 12292
  42.2 37.6 %copy-start.17 = (f32[4,256]{1,0:T(4,128)S(1)}, f32[4,256]{1,0:T(4,128)}, u32[]{:S(2)}) copy-start(f32[4,256]{1,0:T(4,128)} %param.26) | copy-start | bytes 12292
  49.1 30.6 %all-to-all-start.2 = ((f16[64,4,512]{2,1,0:T(4,128)(2,1)}), f16[64,4,512]{2,1,0:T(4,128)(2,1)S(1)}, u32[]{:S(2)}, u32[]{:S(2)}) async-start(f16[64,4,512]{2,1,0:T(4,128)(2,1)} %fusion.14), calls=%async_computation.2 | async-start | bytes 524288 | tf_op jit(solution)/shard_map/all_to_all | solution.py:101
  80.7 18.4 %all-to-all-start.3 = ((f16[64,4,512]{2,1,0:T(4,128)(2,1)}), f16[64,4,512]{2,1,0:T(4,128)(2,1)S(1)}, u32[]{:S(2)}, u32[]{:S(2)}) async-start(f16[64,4,512]{2,1,0:T(4,128)(2,1)} %broadcast_in_dim.5), calls=%async_computation.3 | async-start | bytes 524288 | tf_op jit(solution)/shard_map/all_to_all | solution.py:47
  85.9 13.2 %copy-start.4 = (f16[2048,512]{1,0:T(8,128)(2,1)}, f16[2048,512]{1,0:T(8,128)(2,1)S(1)}, u32[]{:S(2)}) copy-start(f16[2048,512]{1,0:T(8,128)(2,1)S(1)} %constant_dynamic-update-slice_fusion) | copy-start | bytes 6291460
  99.1 54.7 %all-to-all-start.4 = ((f16[64,32,512]{2,1,0:T(8,128)(2,1)}), f16[64,32,512]{2,1,0:T(8,128)(2,1)S(1)}, u32[]{:S(2)}, u32[]{:S(2)}) async-start(f16[64,32,512]{2,1,0:T(8,128)(2,1)} %bitcast.32), calls=%async_computation.4 | async-start | bytes 4194304 | tf_op jit(solution)/shard_map/all_to_all | solution.py:23
  108.5 4.5 %copy-start.3 = (bf16[2048,256]{1,0:T(8,128)(2,1)S(1)}, bf16[2048,256]{1,0:T(8,128)(2,1)}, u32[]{:S(2)}) copy-start(bf16[2048,256]{1,0:T(8,128)(2,1)} %param.23) | copy-start | bytes 3145732
  155.5 5.2 %copy-start.2 = (f32[256,2048]{1,0:T(8,128)S(1)}, f32[256,2048]{1,0:T(8,128)}, u32[]{:S(2)}) copy-start(f32[256,2048]{1,0:T(8,128)} %fusion.31) | copy-start | bytes 6291460
  163.5 2.4 %copy-start.1 = (f32[256,2048]{1,0:T(8,128)S(1)}, f32[256,2048]{1,0:T(8,128)}, u32[]{:S(2)}) copy-start(f32[256,2048]{1,0:T(8,128)} %fusion.25) | copy-start | bytes 6291460
